TPU v7x, 32 devices: a whole 2x2x4 slice. The times are simulated.
32 devices in a mesh: grp: 2 (over y), kv: 4 (over z), tp: 4 (over x, core).
Axes of the slice: x: 2, y: 2, z: 4, core: 2. Of those that a mesh axis runs over, the one named last changes fastest.
Arguments:
- tokens: bfloat16 [32, 4096], P('grp', 'kv'), parts along dimension 0, may hold values from -40 to 40
- lengths: int32 [32], P(('grp', 'kv')), parts along dimension 0, may hold values from 1 to 6, 40 in all
- conv_state_x: bfloat16 [32, 3, 4096], P(('grp', 'kv'), None, 'tp'), parts along dimension 0, may hold values from -6 to 6
- conv_state_bc: bfloat16 [32, 3, 2, 1024], P(('grp', 'kv'), None, None, 'tp'), parts along dimension 0, may hold values from -6 to 6
- ssm_state: float32 [32, 64, 64, 128], P(('grp', 'kv'), 'tp'), parts along dimension 0, may hold values from -0.6 to 0.6
- norm_gain: bfloat16 [4096], P('kv'), may hold values from 0.099609375 to 1.8984375
- w_gate: bfloat16 [4096, 4096], P('kv', 'tp'), may hold values from -0.09375 to 0.09375
- w_value: bfloat16 [4096, 4096], P('kv', 'tp'), may hold values from -0.09375 to 0.09375
- w_key: bfloat16 [4096, 1024], P('kv', 'tp'), may hold values from -0.09375 to 0.09375
- w_query: bfloat16 [4096, 1024], P('kv', 'tp'), may hold values from -0.09375 to 0.09375
- w_step: bfloat16 [4096, 64], P('kv', 'tp'), may hold values from -0.09375 to 0.09375
- step_bias: float32 [64], P('tp'), may hold values from -2 to 0
- decay_log: float32 [64], P('tp'), may hold values from -2 to 1
- conv_x: bfloat16 [4, 4096], P(None, 'tp'), may hold values from -3 to 3
- conv_bc: bfloat16 [4, 2, 1024], P(None, None, 'tp'), may hold values from -3 to 3
- inner_gain: bfloat16 [4096], P('tp'), may hold values from 0.099609375 to 1.8984375
- w_out: bfloat16 [4096, 4096], P('tp', 'kv'), may hold values from -0.09375 to 0.09375
- mlp_gain: bfloat16 [4096], P('kv'), may hold values from 0.099609375 to 1.8984375
- w_up: bfloat16 [4096, 16384], P('kv', 'tp'), may hold values from -0.09375 to 0.09375
- w_down: bfloat16 [16384, 4096], P('tp', 'kv'), may hold values from -0.046875 to 0.046875
Outputs:
- layer_out: bfloat16 [32, 4096], P('grp', 'kv'), parts along dimension 0
- next_state: float32 [32, 64, 64, 128], P(('grp', 'kv'), 'tp'), parts along dimension 0
There are 2 independent parts, one for each index of `grp`. A program takes and returns all parts, laid end to end along the dimension named above; an argument that names none is the same for every part. Nothing has to cross between parts.
All inputs are finite; a program needn't handle non-finite values. No bound on the sum of `lengths` on one device may be relied on, other than what follows from the above.
Results may differ from a plain program's by a relative error of at most 0.008.
Values may be sent and summed in bfloat16 or wider, within the bound.
A program may use at most 64 MiB of HBM per device.

v0:
```python
import jax
import jax.numpy as jnp
from jax import lax
from jax.sharding import PartitionSpec as P

D = 4096
HEAD_DIM = 64
STATE = 128
CONV_WIDTH = 4
INNER = 4096
epsilon = 1e-06


def causal_conv(state_rows, newest, conv_weights):
    extended = jnp.concatenate([state_rows, newest[:, None]], axis=1)
    conv_sum = extended[:, 0] * conv_weights[0].astype(jnp.float32)
    for offset in range(1, conv_weights.shape[0]):
        conv_sum = conv_sum + extended[:, offset] * conv_weights[offset].astype(jnp.float32)
    return jax.nn.silu(conv_sum)


def product(left, right):
    return jnp.dot(left, right, preferred_element_type=jnp.float32)


def per_device(
    tokens,
    lengths,
    conv_state_x,
    conv_state_bc,
    ssm_state,
    norm_gain,
    w_gate,
    w_value,
    w_key,
    w_query,
    w_step,
    step_bias,
    decay_log,
    conv_x,
    conv_bc,
    inner_gain,
    w_out,
    mlp_gain,
    w_up,
    w_down,
):
    head_count = w_step.shape[1]
    group_count = w_key.shape[1] // STATE
    per_group = head_count // group_count
    widened = tokens.astype(jnp.float32)
    scaled = (widened * norm_gain.astype(jnp.float32)).astype(jnp.bfloat16)
    gate_raw, value_raw, key_raw, query_raw, step_raw, squares = (
        lax.psum_scatter(product(scaled, w_gate), "kv", scatter_dimension=0, tiled=True),
        lax.psum_scatter(product(scaled, w_value), "kv", scatter_dimension=0, tiled=True),
        lax.psum_scatter(product(scaled, w_key), "kv", scatter_dimension=0, tiled=True),
        lax.psum_scatter(product(scaled, w_query), "kv", scatter_dimension=0, tiled=True),
        lax.psum_scatter(product(scaled, w_step), "kv", scatter_dimension=0, tiled=True),
        lax.psum_scatter(jnp.sum(widened * widened, axis=1), "kv", scatter_dimension=0, tiled=True),
    )
    seq_count = gate_raw.shape[0]
    inverse = lax.rsqrt(squares / D + epsilon)[:, None]
    row_live = (
        jnp.arange(CONV_WIDTH - 1, dtype=jnp.int32)[None, :] >= CONV_WIDTH - 1 - lengths[:, None]
    ).astype(jnp.float32)
    live_x = conv_state_x.astype(jnp.float32) * row_live[:, :, None]
    live_bc = conv_state_bc.astype(jnp.float32) * row_live[:, :, None, None]
    mixed_values = causal_conv(live_x, value_raw * inverse, conv_x).reshape(
        seq_count, head_count, HEAD_DIM
    )
    key_query = causal_conv(
        live_bc, jnp.stack([key_raw * inverse, query_raw * inverse], axis=1), conv_bc
    )
    key_heads = jnp.repeat(
        key_query[:, 0].reshape(seq_count, group_count, STATE), per_group, axis=1
    )
    query_heads = jnp.repeat(
        key_query[:, 1].reshape(seq_count, group_count, STATE), per_group, axis=1
    )
    step_size = jax.nn.softplus(step_raw * inverse + step_bias)
    rate_now = -jnp.exp(decay_log) * step_size
    next_state = (
        ssm_state * jnp.exp(rate_now)[:, :, None, None]
        + (step_size[:, :, None] * mixed_values)[:, :, :, None] * key_heads[:, :, None, :]
    )
    mixer_y = jnp.einsum(
        "bhpn,bhn->bhp", next_state, query_heads, precision=lax.Precision.HIGHEST
    ).reshape(seq_count, head_count * HEAD_DIM)
    gated_rows = mixer_y * jax.nn.silu(gate_raw * inverse)
    gated_low = (gated_rows * inner_gain.astype(jnp.float32)).astype(jnp.bfloat16)
    all_low, all_squares = (
        lax.all_gather(gated_low, "kv", axis=0, tiled=True),
        lax.all_gather(
            jnp.sum(gated_rows * gated_rows, axis=1).astype(jnp.bfloat16), "kv", axis=0, tiled=True
        ).astype(jnp.float32),
    )
    out_sum, gated_total = lax.psum((product(all_low, w_out), all_squares), "tp")
    residual = (widened + out_sum * lax.rsqrt(gated_total / INNER + epsilon)[:, None]).astype(
        jnp.bfloat16
    )
    residual_wide = residual.astype(jnp.float32)
    hidden_low = (residual_wide * mlp_gain.astype(jnp.float32)).astype(jnp.bfloat16)
    row_squares = jnp.sum(residual_wide * residual_wide, axis=1)
    up_sum, square_sum = lax.psum((product(hidden_low, w_up), row_squares), "kv")
    activation = jnp.square(
        jax.nn.relu(up_sum * lax.rsqrt(square_sum / D + epsilon)[:, None])
    ).astype(jnp.bfloat16)
    down_sum = lax.psum(product(activation, w_down), "tp")
    layer_out = (residual_wide + down_sum).astype(jnp.bfloat16)
    return (layer_out, next_state)


def solution(mesh):
    return jax.shard_map(
        per_device,
        mesh=mesh,
        in_specs=(
            P("grp", "kv"),
            P(("grp", "kv")),
            P(("grp", "kv"), None, "tp"),
            P(("grp", "kv"), None, None, "tp"),
            P(("grp", "kv"), "tp", None, None),
            P("kv"),
            P("kv", "tp"),
            P("kv", "tp"),
            P("kv", "tp"),
            P("kv", "tp"),
            P("kv", "tp"),
            P("tp"),
            P("tp"),
            P(None, "tp"),
            P(None, None, "tp"),
            P("tp"),
            P("tp", "kv"),
            P("kv"),
            P("kv", "tp"),
            P("tp", "kv"),
        ),
        out_specs=(P("grp", "kv"), P(("grp", "kv"), "tp", None, None)),
        check_vma=False,
    )
```

profile of v0, /device:TPU:0, one launch (start us, length us, event | category | flops | bytes accessed | tf_op | source)
XLA Modules:
  0.0 207.7 jit_solution(14826090005879602014)
XLA Ops:
  7.2 0.0 copy-start
  7.2 0.0 copy-start.3
  7.2 0.0 all-reduce.20.cloned.1.call-start
  7.2 0.0 copy-start.2
  7.2 0.8 convert_element_type.73
  8.1 0.7 copy-done
  8.8 0.0 copy-start.4
  8.8 0.0 copy-start.5
  8.8 1.9 fusion.26
  10.7 0.0 copy-done.3
  10.7 0.0 copy-done.2
  10.7 0.0 copy-start.9
  10.7 0.0 copy-start.8
  10.7 0.0 copy-start.14
  10.7 1.0 fusion.20
  11.7 0.0 all-reduce.20.cloned.1.call-update
  11.8 0.0 all-reduce.14.cloned.1.call-start
  11.8 0.1 fusion.4
  12.0 0.0 copy-done.15
  12.0 0.0 copy-done.16
  12.0 0.0 copy-done.6
  12.0 0.1 fusion.28
  12.2 0.0 copy-done.4
  12.2 0.2 fusion.24
  12.3 0.2 fusion.22
  12.6 0.7 fusion.47
  13.9 21.3 %all-reduce.7 = (f32[16,256]{1,0:T(8,128)S(1)}, f32[16]{0:T(128)S(1)}, f32[16,256]{1,0:T(8,128)S(1)}, f32[16,16]{1,0:T(8,128)S(1)}) all-reduce(f32[16,256]{1,0:T(8,128)S(1)} %fusion.22, f32[16]{0:T(128)S(1)} %fusion.4, f32[16,256]{1,0:T(8,128)S(1)} %fusion.24, ...), channel_id=6, replica_groups=mesh['grp'=2,'kv'=4,'tp'=4] {'kv'}, use_global_device_ids=true, to_apply=%region_5.0.clone | all-reduce | flops 8464 | bytes 67712
  35.2 0.1 fusion.42
  35.3 0.1 convert_multiply_fusion.5
  35.4 0.1 fusion.38
  35.5 0.1 convert_multiply_fusion.4
  36.3 0.1 multiply_exponential_fusion
  36.4 13.2 %all-reduce.20.cloned.1.call-done = (f32[16,1024]{1,0:T(8,128)}, f32[16,1024]{1,0:T(8,128)}) async-done(((f32[16,1024]{1,0:T(8,128)}, f32[16,1024]{1,0:T(8,128)}), (f32[16,1024]{1,0:T(8,128)}, f32[16,1024]{1,0:T(8,128)})) %all-reduce.20.cloned.1.call-update) | async-done | bytes 131088
  49.5 0.8 divide_multiply_fusion.1
  50.4 0.1 reshape.72
  50.5 0.1 broadcast_multiply_fusion
  50.6 2.1 multiply_add_fusion
  52.6 0.0 copy-start.1
  52.6 0.0 copy-start.11
  52.6 0.0 copy-start.12
  52.7 1.3 copy-done.1
  53.9 3.3 %fusion.48 = f32[4,16,1,64]{3,2,1,0:T(1,128)S(1)} fusion(f32[4,16,64,128]{3,2,1,0:T(8,128)S(1)} %multiply_add_fusion, f32[4,16,128,1]{2,3,1,0:T(1,128)S(1)} %bitcast.104), kind=kOutput, calls=%fused_computation.85 | convolution fusion | flops 6291456 | bytes 2146304 | tf_op jit(solution)/shard_map/bhpn,bhn->bhp/dot_general | solution.py:86
  57.3 0.1 reshape.74
  57.4 1.0 multiply_reduce_fusion
  58.3 0.2 dynamic-update-slice
  58.6 0.0 copy-done.11
  58.6 10.6 %all-reduce = bf16[16]{0:T(256)(128)(2,1)S(1)} all-reduce(bf16[16]{0:T(256)(128)(2,1)S(1)} %dynamic-update-slice), channel_id=1, replica_groups=mesh['grp'=2,'kv'=4,'tp'=4] {'kv'}, use_global_device_ids=true, to_apply=%add | all-reduce | flops 16 | bytes 64
  69.2 0.0 copy-done.12
  69.2 5.7 %psum.36 = f32[16]{0:T(128)S(1)} all-reduce(bf16[16]{0:T(256)(128)(2,1)S(1)} %all-reduce), channel_id=1, replica_groups=mesh['grp'=2,'kv'=4,'tp'=4] {'tp'}, use_global_device_ids=true, to_apply=%region_9.10 | all-reduce | flops 16 | bytes 96 | tf_op jit(solution)/shard_map/psum | solution.py:97
  74.9 13.1 %all-gather = bf16[4,4,1024]{2,1,0:T(4,128)(2,1)S(1)} all-gather(bf16[1,4,1024]{2,1,0:T(4,128)(2,1)S(1)} %fusion.30), channel_id=1, replica_groups=mesh['grp'=2,'kv'=4,'tp'=4] {'kv'}, dimensions={0}, use_global_device_ids=true | all-gather | bytes 40960 | tf_op jit(solution)/shard_map/all_gather | solution.py:92
  88.0 2.6 %fusion.49 = f32[16,1024]{1,0:T(8,128)} fusion(bf16[16,1024]{1,0:T(8,128)(2,1)S(1)} %reshape.87, bf16[1024,1024]{1,0:T(8,128)(2,1)} %param.36), kind=kOutput, calls=%fused_computation.86 | convolution fusion | flops 33554432 | bytes 2195456 | tf_op jit(solution)/shard_map/dot_general | solution.py:23
  90.6 0.0 all-reduce.14.cloned.1.call-update
  90.7 0.0 all-reduce.16.cloned.1.call-start
  90.7 30.0 %all-reduce.14.cloned.1.call-done = f32[16,1024]{1,0:T(8,128)} async-done(((f32[16,1024]{1,0:T(8,128)}), f32[16,1024]{1,0:T(8,128)}) %all-reduce.14.cloned.1.call-update) | async-done | bytes 65552 | tf_op jit(solution)/shard_map/psum | solution.py:97
  120.7 1.0 fusion.7
  121.7 5.3 %fusion.9 = f32[16,4096]{1,0:T(8,128)} fusion(bf16[1024,4096]{1,0:T(8,128)(2,1)} %param.38, bf16[16,1024]{1,0:T(8,128)(2,1)S(1)} %get-tuple-element.9, f32[1024]{0:T(1024)S(1)} %convert_element_type.84), kind=kOutput, calls=%fused_computation.18 | convolution fusion | flops 134266880 | bytes 8687616 | tf_op jit(solution)/shard_map/dot_general | solution.py:23
  127.0 0.0 all-reduce.16.cloned.1.call-update
  127.0 0.0 all-reduce.18.cloned.1.call-start
  127.1 11.8 %psum.38 = f32[16]{0:T(128)S(1)} all-reduce(f32[16]{0:T(128)S(1)} %get-tuple-element.8), channel_id=1, replica_groups=mesh['grp'=2,'kv'=4,'tp'=4] {'kv'}, use_global_device_ids=true, to_apply=%region_12.13 | all-reduce | flops 16 | bytes 128 | tf_op jit(solution)/shard_map/psum | solution.py:104
  138.9 23.9 %all-reduce.16.cloned.1.call-done = f32[16,4096]{1,0:T(8,128)} async-done(((f32[16,4096]{1,0:T(8,128)}), f32[16,4096]{1,0:T(8,128)}) %all-reduce.16.cloned.1.call-update) | async-done | bytes 262160 | tf_op jit(solution)/shard_map/psum | solution.py:104
  162.8 5.3 %fusion = f32[16,1024]{1,0:T(8,128)} fusion(bf16[4096,1024]{1,0:T(8,128)(2,1)} %param.39, f32[16,4096]{1,0:T(8,128)} %all-reduce.16.cloned.1.call-done, f32[16]{0:T(128)S(1)} %add_rsqrt_fusion), kind=kOutput, calls=%fused_computation.2 | convolution fusion | flops 134479872 | bytes 8716352 | tf_op jit(solution)/shard_map/dot_general | solution.py:23
  168.1 0.0 all-reduce.18.cloned.1.call-update
  168.2 31.6 %all-reduce.18.cloned.1.call-done = f32[16,1024]{1,0:T(8,128)} async-done(((f32[16,1024]{1,0:T(8,128)}), f32[16,1024]{1,0:T(8,128)}) %all-reduce.18.cloned.1.call-update) | async-done | bytes 65552 | tf_op jit(solution)/shard_map/psum | solution.py:108
  199.7 1.5 fusion.8
  (31 shorter events, 0.2 us)
Async XLA Ops:
  7.2 1.6 copy-start
  7.2 3.5 %copy-start.3 = (bf16[16,1024]{1,0:T(8,128)(2,1)S(1)}, bf16[16,1024]{1,0:T(8,128)(2,1)}, u32[]{:S(2)}) copy-start(bf16[16,1024]{1,0:T(8,128)(2,1)} %param.20) | copy-start | bytes 98308
  7.2 42.3 %all-reduce.20.cloned.1.call-start = ((), (), s32[]{:S(2)}) async-start(), calls=%async_computation.3 | async-start | bytes 262144
  7.2 3.4 %copy-start.2 = (bf16[1024,1024]{1,0:T(8,128)(2,1)S(1)}, bf16[1024,1024]{1,0:T(8,128)(2,1)}, u32[]{:S(2)}) copy-start(bf16[1024,1024]{1,0:T(8,128)(2,1)} %param.26) | copy-start | bytes 6291460
  8.8 3.2 %copy-start.15 = (s32[4]{0:T(128)S(1)}, s32[4]{0:T(128)}, u32[]{:S(2)}) copy-start(s32[4]{0:T(128)} %param.21) | copy-start | bytes 52
  8.8 3.2 %copy-start.16 = (f32[16]{0:T(128)S(1)}, f32[16]{0:T(128)}, u32[]{:S(2)}) copy-start(f32[16]{0:T(128)} %param.32) | copy-start | bytes 196
  8.8 3.2 %copy-start.6 = (bf16[1024,16]{0,1:T(8,128)(2,1)S(1)}, bf16[1024,16]{0,1:T(8,128)(2,1)}, u32[]{:S(2)}) copy-start(bf16[1024,16]{0,1:T(8,128)(2,1)} %param.30) | copy-start | bytes 98308
  8.8 3.4 %copy-start.10 = (bf16[4,2,256]{2,1,0:T(2,128)(2,1)S(1)}, bf16[4,2,256]{2,1,0:T(2,128)(2,1)}, u32[]{:S(2)}) copy-start(bf16[4,2,256]{2,1,0:T(2,128)(2,1)} %param.34) | copy-start | bytes 12292
  8.8 3.4 %copy-start.4 = (bf16[1024,256]{1,0:T(8,128)(2,1)S(1)}, bf16[1024,256]{1,0:T(8,128)(2,1)}, u32[]{:S(2)}) copy-start(bf16[1024,256]{1,0:T(8,128)(2,1)} %param.28) | copy-start | bytes 1572868
  8.8 3.5 %copy-start.5 = (bf16[1024,256]{1,0:T(8,128)(2,1)S(1)}, bf16[1024,256]{1,0:T(8,128)(2,1)}, u32[]{:S(2)}) copy-start(bf16[1024,256]{1,0:T(8,128)(2,1)} %param.29) | copy-start | bytes 1572868
  10.7 1.8 copy-start.7
  10.7 1.9 copy-start.13
  10.7 24.6 %copy-start.9 = (bf16[4,3,2,256]{3,2,1,0:T(2,128)(2,1)S(1)}, bf16[4,3,2,256]{3,2,1,0:T(2,128)(2,1)}, u32[]{:S(2)}) copy-start(bf16[4,3,2,256]{3,2,1,0:T(2,128)(2,1)} %param.23) | copy-start | bytes 36868
  10.7 24.8 %copy-start.8 = (bf16[4,3,1024]{2,0,1:T(4,128)(2,1)S(1)}, bf16[4,3,1024]{2,0,1:T(4,128)(2,1)}, u32[]{:S(2)}) copy-start(bf16[4,3,1024]{2,0,1:T(4,128)(2,1)} %param.22) | copy-start | bytes 73732
  10.7 25.6 %copy-start.14 = (f32[16]{0:T(128)S(1)}, f32[16]{0:T(128)}, u32[]{:S(2)}) copy-start(f32[16]{0:T(128)} %param.31) | copy-start | bytes 196
  11.8 108.9 %all-reduce.14.cloned.1.call-start = ((), (), s32[]{:S(2)}) async-start(), calls=%async_computation | async-start | bytes 131072 | tf_op jit(solution)/shard_map/psum | solution.py:97
  52.6 1.3 copy-start.1
  52.6 6.0 %copy-start.11 = (bf16[1024]{0:T(1024)(128)(2,1)S(1)}, bf16[1024]{0:T(1024)(128)(2,1)}, u32[]{:S(2)}) copy-start(bf16[1024]{0:T(1024)(128)(2,1)} %param.35) | copy-start | bytes 6148
  52.6 16.6 %copy-start.12 = (bf16[1024]{0:T(1024)(128)(2,1)S(1)}, bf16[1024]{0:T(1024)(128)(2,1)}, u32[]{:S(2)}) copy-start(bf16[1024]{0:T(1024)(128)(2,1)} %param.37) | copy-start | bytes 6148
  90.7 72.2 %all-reduce.16.cloned.1.call-start = ((), (), s32[]{:S(2)}) async-start(), calls=%async_computation.1 | async-start | bytes 524288 | tf_op jit(solution)/shard_map/psum | solution.py:104
  127.0 72.7 %all-reduce.18.cloned.1.call-start = ((), (), s32[]{:S(2)}) async-start(), calls=%async_computation.2 | async-start | bytes 131072 | tf_op jit(solution)/shard_map/psum | solution.py:108
Sparse Core Ops, SparseCore 0:
  11.9 37.6 all-reduce.19
  90.8 29.8 all-reduce.13
  127.2 35.5 all-reduce.15
  168.3 31.3 all-reduce.17
where the time goes:
time: 208 us
  waiting for transfers between devices  98.7 us (47%)
  blocking collectives  62.5 us (30%)
  matrix products  19.9 us (10%)
  between operations  15.4 us (7%)
  other arithmetic  7.87 us (4%)
  local copies, waits for them, and re-layouts  3.2 us (2%)
    unnamed x2, blocking collectives  31.9 us
    psum x1, waiting for transfers between devices, per_device(): down_sum = lax.psum(product(activation, w_down), 'tp')  31.6 us
    psum x1, waiting for transfers between devices, per_device(): lax.psum((product(all_low, w_out), all_squares), 'tp')  30 us
    psum x1, waiting for transfers between devices, per_device(): lax.psum((product(hidden_low, w_up), row_squares), 'kv')  23.9 us
    dot_general x8, matrix products, product(): return jnp.dot(left, right, preferred_element_type=jnp.float32)  16.6 us
    unnamed x5, waiting for transfers between devices  13.2 us
    all_gather x1, blocking collectives, per_device(): lax.all_gather(gated_low, 'kv', axis=0, tiled=True)  13.1 us
    psum x1, blocking collectives, per_device(): lax.psum((product(hidden_low, w_up), row_squares), 'kv')  11.8 us
  transfers between devices with their start and end apart: 4, of which 4 were waited for; matrix products, arithmetic and copies ran while one was open for 1% of the time, Pallas kernels for 0%

commit v1 on v0

--- a/solution.py
+++ b/solution.py
@@ -105,7 +105,9 @@
     activation = jnp.square(
         jax.nn.relu(up_sum * lax.rsqrt(square_sum / D + epsilon)[:, None])
     ).astype(jnp.bfloat16)
-    down_sum = lax.psum(product(activation, w_down), "tp")
+    x = product(activation, w_down)
+    parts = lax.all_gather(x, "tp", axis=0, tiled=False)
+    down_sum = parts.sum(axis=0)
     layer_out = (residual_wide + down_sum).astype(jnp.bfloat16)
     return (layer_out, next_state)
 

time: 208 us -> 181 us (0.87)
  waiting for transfers between devices: 98.7 us -> 67.2 us
  blocking collectives: 62.5 us -> 68.3 us
    psum x1 -> x0, waiting for transfers between devices: 31.6 us -> none  [per_device(): down_sum = lax.psum(product(activation, w_down), 'tp')]
    all_gather x0 -> x1, blocking collectives: none -> 5.77 us  [per_device(): parts = lax.all_gather(x, 'tp', axis=0, tiled=False)]
    unnamed x5 -> x4, waiting for transfers between devices: 13.2 us -> 13.3 us
  transfers between devices with their start and end apart: 4 -> 3, of which waited for: 4 -> 3; matrix products, arithmetic and copies ran while one was open for 1% -> 1% of each run, Pallas kernels for 0% -> 0%
where the time goes in v1:
time: 181 us; the launch traced here: 180 us
  blocking collectives  68.3 us (38%)
  waiting for transfers between devices  67.2 us (37%)
  matrix products  19.3 us (11%)
  between operations  15.3 us (8%)
  other arithmetic  7.05 us (4%)
  local copies, waits for them, and re-layouts  3.15 us (2%)
    unnamed x2, blocking collectives  31.9 us
    psum x1, waiting for transfers between devices, per_device(): lax.psum((product(all_low, w_out), all_squares), 'tp')  30 us
    psum x1, waiting for transfers between devices, per_device(): lax.psum((product(hidden_low, w_up), row_squares), 'kv')  24 us
    dot_general x8, matrix products, product(): return jnp.dot(left, right, preferred_element_type=jnp.float32)  16 us
    unnamed x4, waiting for transfers between devices  13.3 us
    all_gather x1, blocking collectives, per_device(): lax.all_gather(gated_low, 'kv', axis=0, tiled=True)  13.1 us
    psum x1, blocking collectives, per_device(): lax.psum((product(hidden_low, w_up), row_squares), 'kv')  11.8 us
    all_gather x1, blocking collectives, per_device(): parts = lax.all_gather(x, 'tp', axis=0, tiled=False)  5.77 us
  transfers between devices with their start and end apart: 3, of which 3 were waited for; matrix products, arithmetic and copies ran while one was open for 1% of the time, Pallas kernels for 0%

profile of v1, /device:TPU:0, one launch (start us, length us, event | category | flops | bytes accessed | tf_op | source)
XLA Modules:
  0.0 180.5 jit_solution(1329660261869002265)
XLA Ops:
  7.2 0.0 copy-start
  7.2 0.0 copy-start.3
  7.2 0.0 all-reduce.17.cloned.1.call-start
  7.2 0.0 copy-start.2
  7.2 0.8 convert_element_type.73
  8.1 0.7 copy-done
  8.8 0.0 copy-start.4
  8.8 0.0 copy-start.5
  8.8 1.9 %fusion.26 = f32[16,1024]{1,0:T(8,128)} fusion(bf16[1024,1024]{1,0:T(8,128)(2,1)S(1)} %copy-done, bf16[16,1024]{1,0:T(8,128)(2,1)} %param.20, f32[1024]{0:T(1024)S(1)} %convert_element_type.73), kind=kOutput, calls=%fused_computation.43 | convolution fusion | flops 33603584 | bytes 2199552 | tf_op jit(solution)/shard_map/dot_general | solution.py:23
  10.7 0.0 copy-done.3
  10.7 0.0 copy-done.2
  10.7 0.0 copy-start.9
  10.7 0.0 copy-start.8
  10.7 0.0 copy-start.14
  10.7 1.0 fusion.20
  11.8 0.0 all-reduce.17.cloned.1.call-update
  11.8 0.0 all-reduce.13.cloned.1.call-start
  11.8 0.1 fusion.4
  12.0 0.0 copy-done.15
  12.0 0.0 copy-done.16
  12.0 0.0 copy-done.6
  12.0 0.1 fusion.28
  12.2 0.0 copy-done.10
  12.2 0.0 copy-done.4
  12.2 0.2 fusion.24
  12.4 0.0 copy-done.5
  12.4 0.2 fusion.22
  12.5 0.0 copy-done.7
  12.6 0.0 copy-done.13
  12.6 0.6 fusion.47
  13.9 21.3 %all-reduce.7 = (f32[16,256]{1,0:T(8,128)S(1)}, f32[16]{0:T(128)S(1)}, f32[16,256]{1,0:T(8,128)S(1)}, f32[16,16]{1,0:T(8,128)S(1)}) all-reduce(f32[16,256]{1,0:T(8,128)S(1)} %fusion.22, f32[16]{0:T(128)S(1)} %fusion.4, f32[16,256]{1,0:T(8,128)S(1)} %fusion.24, ...), channel_id=7, replica_groups=mesh['grp'=2,'kv'=4,'tp'=4] {'kv'}, use_global_device_ids=true, to_apply=%region_5.0.clone | all-reduce | flops 8464 | bytes 67712
  35.1 0.1 fusion.42
  35.2 0.1 convert_multiply_fusion.5
  35.3 0.1 fusion.38
  35.5 0.1 convert_multiply_fusion.4
  36.2 0.1 multiply_exponential_fusion
  36.3 13.2 %all-reduce.17.cloned.1.call-done = (f32[16,1024]{1,0:T(8,128)}, f32[16,1024]{1,0:T(8,128)}) async-done(((f32[16,1024]{1,0:T(8,128)}, f32[16,1024]{1,0:T(8,128)}), (f32[16,1024]{1,0:T(8,128)}, f32[16,1024]{1,0:T(8,128)})) %all-reduce.17.cloned.1.call-update) | async-done | bytes 131088
  49.5 0.8 divide_multiply_fusion.1
  50.4 0.1 reshape.72
  50.5 0.1 broadcast_multiply_fusion
  50.5 2.1 %multiply_add_fusion = f32[4,16,64,128]{3,2,1,0:T(8,128)S(1)} fusion(f32[4,16,64,128]{3,2,1,0:T(8,128)} %param.24, f32[4,16,128]{2,1,0:T(8,128)S(1)} %broadcast_bitcast_fusion, f32[4,16,64]{2,1,0:T(8,128)S(1)} %broadcast_multiply_fusion, f32[4,16]{1,0:T(4,128)S(1)} %get-tuple-element.12), kind=kLoop, calls=%fused_computation | loop fusion | flops 1572864 | bytes 4243712 | tf_op jit(solution)/shard_map/add | solution.py:83
  52.6 0.0 copy-start.1
  52.6 0.0 copy-start.11
  52.6 0.0 copy-start.12
  52.6 1.3 copy-done.1
  53.9 3.3 %fusion.48 = f32[4,16,1,64]{3,2,1,0:T(1,128)S(1)} fusion(f32[4,16,64,128]{3,2,1,0:T(8,128)S(1)} %multiply_add_fusion, f32[4,16,128,1]{2,3,1,0:T(1,128)S(1)} %bitcast.106), kind=kOutput, calls=%fused_computation.85 | convolution fusion | flops 6291456 | bytes 2146304 | tf_op jit(solution)/shard_map/bhpn,bhn->bhp/dot_general | solution.py:86
  57.3 0.1 reshape.74
  57.4 1.0 multiply_reduce_fusion
  58.3 0.2 dynamic-update-slice
  58.6 10.6 %all-reduce = bf16[16]{0:T(256)(128)(2,1)S(1)} all-reduce(bf16[16]{0:T(256)(128)(2,1)S(1)} %dynamic-update-slice), channel_id=1, replica_groups=mesh['grp'=2,'kv'=4,'tp'=4] {'kv'}, use_global_device_ids=true, to_apply=%add | all-reduce | flops 16 | bytes 64
  69.2 5.7 %psum.29 = f32[16]{0:T(128)S(1)} all-reduce(bf16[16]{0:T(256)(128)(2,1)S(1)} %all-reduce), channel_id=1, replica_groups=mesh['grp'=2,'kv'=4,'tp'=4] {'tp'}, use_global_device_ids=true, to_apply=%region_9.10 | all-reduce | flops 16 | bytes 96 | tf_op jit(solution)/shard_map/psum | solution.py:97
  74.9 13.1 %all-gather.1 = bf16[4,4,1024]{2,1,0:T(4,128)(2,1)S(1)} all-gather(bf16[1,4,1024]{2,1,0:T(4,128)(2,1)S(1)} %fusion.30), channel_id=1, replica_groups=mesh['grp'=2,'kv'=4,'tp'=4] {'kv'}, dimensions={0}, use_global_device_ids=true | all-gather | bytes 40960 | tf_op jit(solution)/shard_map/all_gather | solution.py:92
  88.0 2.6 %fusion.49 = f32[16,1024]{1,0:T(8,128)} fusion(bf16[16,1024]{1,0:T(8,128)(2,1)S(1)} %reshape.88, bf16[1024,1024]{1,0:T(8,128)(2,1)} %param.36), kind=kOutput, calls=%fused_computation.86 | convolution fusion | flops 33554432 | bytes 2195456 | tf_op jit(solution)/shard_map/dot_general | solution.py:23
  90.6 0.0 all-reduce.13.cloned.1.call-update
  90.7 0.0 all-reduce.15.cloned.1.call-start
  90.7 30.0 %all-reduce.13.cloned.1.call-done = f32[16,1024]{1,0:T(8,128)} async-done(((f32[16,1024]{1,0:T(8,128)}), f32[16,1024]{1,0:T(8,128)}) %all-reduce.13.cloned.1.call-update) | async-done | bytes 65552 | tf_op jit(solution)/shard_map/psum | solution.py:97
  120.7 1.0 fusion.7
  121.7 5.3 %fusion.9 = f32[16,4096]{1,0:T(8,128)} fusion(bf16[1024,4096]{1,0:T(8,128)(2,1)} %param.38, bf16[16,1024]{1,0:T(8,128)(2,1)S(1)} %get-tuple-element.9, f32[1024]{0:T(1024)S(1)} %convert_element_type.84), kind=kOutput, calls=%fused_computation.18 | convolution fusion | flops 134266880 | bytes 8687616 | tf_op jit(solution)/shard_map/dot_general | solution.py:23
  127.0 0.0 all-reduce.15.cloned.1.call-update
  127.1 11.8 %psum.31 = f32[16]{0:T(128)S(1)} all-reduce(f32[16]{0:T(128)S(1)} %get-tuple-element.8), channel_id=1, replica_groups=mesh['grp'=2,'kv'=4,'tp'=4] {'kv'}, use_global_device_ids=true, to_apply=%region_12.13 | all-reduce | flops 16 | bytes 128 | tf_op jit(solution)/shard_map/psum | solution.py:104
  138.9 24.0 %all-reduce.15.cloned.1.call-done = f32[16,4096]{1,0:T(8,128)} async-done(((f32[16,4096]{1,0:T(8,128)}), f32[16,4096]{1,0:T(8,128)}) %all-reduce.15.cloned.1.call-update) | async-done | bytes 262160 | tf_op jit(solution)/shard_map/psum | solution.py:104
  162.8 4.7 %fusion = f32[16,1024]{1,0:T(8,128)S(1)} fusion(bf16[4096,1024]{1,0:T(8,128)(2,1)} %param.39, f32[16,4096]{1,0:T(8,128)} %all-reduce.15.cloned.1.call-done, f32[16]{0:T(128)S(1)} %add_rsqrt_fusion), kind=kOutput, calls=%fused_computation.2 | convolution fusion | flops 134479872 | bytes 8716352 | tf_op jit(solution)/shard_map/dot_general | solution.py:23
  167.5 5.8 %all-gather = f32[64,1024]{1,0:T(8,128)S(1)} all-gather(f32[16,1024]{1,0:T(8,128)S(1)} %fusion), channel_id=2, replica_groups=mesh['grp'=2,'kv'=4,'tp'=4] {'tp'}, dimensions={0}, use_global_device_ids=true | all-gather | bytes 327680 | tf_op jit(solution)/shard_map/all_gather | solution.py:109
  173.3 0.6 fusion.8
  (30 shorter events, 0.2 us)
Async XLA Ops:
  7.2 1.6 copy-start
  7.2 3.5 %copy-start.3 = (bf16[16,1024]{1,0:T(8,128)(2,1)S(1)}, bf16[16,1024]{1,0:T(8,128)(2,1)}, u32[]{:S(2)}) copy-start(bf16[16,1024]{1,0:T(8,128)(2,1)} %param.20) | copy-start | bytes 98308
  7.2 42.3 %all-reduce.17.cloned.1.call-start = ((), (), s32[]{:S(2)}) async-start(), calls=%async_computation.2 | async-start | bytes 262144
  7.2 3.4 %copy-start.2 = (bf16[1024,1024]{1,0:T(8,128)(2,1)S(1)}, bf16[1024,1024]{1,0:T(8,128)(2,1)}, u32[]{:S(2)}) copy-start(bf16[1024,1024]{1,0:T(8,128)(2,1)} %param.26) | copy-start | bytes 6291460
  8.8 3.2 %copy-start.15 = (s32[4]{0:T(128)S(1)}, s32[4]{0:T(128)}, u32[]{:S(2)}) copy-start(s32[4]{0:T(128)} %param.21) | copy-start | bytes 52
  8.8 3.2 %copy-start.16 = (f32[16]{0:T(128)S(1)}, f32[16]{0:T(128)}, u32[]{:S(2)}) copy-start(f32[16]{0:T(128)} %param.32) | copy-start | bytes 196
  8.8 3.2 %copy-start.6 = (bf16[1024,16]{0,1:T(8,128)(2,1)S(1)}, bf16[1024,16]{0,1:T(8,128)(2,1)}, u32[]{:S(2)}) copy-start(bf16[1024,16]{0,1:T(8,128)(2,1)} %param.30) | copy-start | bytes 98308
  8.8 3.4 %copy-start.10 = (bf16[4,2,256]{2,1,0:T(2,128)(2,1)S(1)}, bf16[4,2,256]{2,1,0:T(2,128)(2,1)}, u32[]{:S(2)}) copy-start(bf16[4,2,256]{2,1,0:T(2,128)(2,1)} %param.34) | copy-start | bytes 12292
  8.8 3.4 %copy-start.4 = (bf16[1024,256]{1,0:T(8,128)(2,1)S(1)}, bf16[1024,256]{1,0:T(8,128)(2,1)}, u32[]{:S(2)}) copy-start(bf16[1024,256]{1,0:T(8,128)(2,1)} %param.28) | copy-start | bytes 1572868
  8.8 3.6 %copy-start.5 = (bf16[1024,256]{1,0:T(8,128)(2,1)S(1)}, bf16[1024,256]{1,0:T(8,128)(2,1)}, u32[]{:S(2)}) copy-start(bf16[1024,256]{1,0:T(8,128)(2,1)} %param.29) | copy-start | bytes 1572868
  10.7 1.9 %copy-start.7 = (bf16[4,1024]{1,0:T(4,128)(2,1)S(1)}, bf16[4,1024]{1,0:T(4,128)(2,1)}, u32[]{:S(2)}) copy-start(bf16[4,1024]{1,0:T(4,128)(2,1)} %param.33) | copy-start | bytes 24580
  10.7 1.9 %copy-start.13 = (u32[32]{0:T(128)S(1)}, u32[32]{0:T(128)}, u32[]{:S(2)}) copy-start(u32[32]{0:T(128)} %constant.29) | copy-start | bytes 388
  10.7 24.5 %copy-start.9 = (bf16[4,3,2,256]{3,2,1,0:T(2,128)(2,1)S(1)}, bf16[4,3,2,256]{3,2,1,0:T(2,128)(2,1)}, u32[]{:S(2)}) copy-start(bf16[4,3,2,256]{3,2,1,0:T(2,128)(2,1)} %param.23) | copy-start | bytes 36868
  10.7 24.8 %copy-start.8 = (bf16[4,3,1024]{2,0,1:T(4,128)(2,1)S(1)}, bf16[4,3,1024]{2,0,1:T(4,128)(2,1)}, u32[]{:S(2)}) copy-start(bf16[4,3,1024]{2,0,1:T(4,128)(2,1)} %param.22) | copy-start | bytes 73732
  10.7 25.5 %copy-start.14 = (f32[16]{0:T(128)S(1)}, f32[16]{0:T(128)}, u32[]{:S(2)}) copy-start(f32[16]{0:T(128)} %param.31) | copy-start | bytes 196
  11.8 108.9 %all-reduce.13.cloned.1.call-start = ((), (), s32[]{:S(2)}) async-start(), calls=%async_computation | async-start | bytes 131072 | tf_op jit(solution)/shard_map/psum | solution.py:97
  52.6 1.3 copy-start.1
  52.6 6.0 %copy-start.11 = (bf16[1024]{0:T(1024)(128)(2,1)S(1)}, bf16[1024]{0:T(1024)(128)(2,1)}, u32[]{:S(2)}) copy-start(bf16[1024]{0:T(1024)(128)(2,1)} %param.35) | copy-start | bytes 6148
  52.6 16.6 %copy-start.12 = (bf16[1024]{0:T(1024)(128)(2,1)S(1)}, bf16[1024]{0:T(1024)(128)(2,1)}, u32[]{:S(2)}) copy-start(bf16[1024]{0:T(1024)(128)(2,1)} %param.37) | copy-start | bytes 6148
  90.7 72.2 %all-reduce.15.cloned.1.call-start = ((), (), s32[]{:S(2)}) async-start(), calls=%async_computation.1 | async-start | bytes 524288 | tf_op jit(solution)/shard_map/psum | solution.py:104
Sparse Core Ops, SparseCore 0:
  11.9 37.5 all-reduce.16
  90.8 29.8 all-reduce.12
  127.2 35.5 all-reduce.14
